TPU v7x, 32 devices: a whole 2x2x4 slice. The times are simulated.
32 devices in a mesh: ep: 4 (over y, x), tp: 8 (over z, core).
Axes of the slice: x: 2, y: 2, z: 4, core: 2. Of those that a mesh axis runs over, the one named last changes fastest.
Arguments:
- tokens: bfloat16 [512, 2048], P('ep'), may hold values from -6 to 6
- conv_state: bfloat16 [512, 3, 2048], P('ep', None, 'tp'), may hold values from -6 to 6
- rec_state: float32 [512, 2048], P('ep', 'tp'), may hold values from -6 to 6
- gate_proj: bfloat16 [2048, 2048], P(None, 'tp'), may hold values from -0.125 to 0.125
- input_proj: bfloat16 [2048, 2048], P(None, 'tp'), may hold values from -0.125 to 0.125
- conv_taps: bfloat16 [4, 2048], P(None, 'tp'), may hold values from -3 to 3
- decay_blocks: bfloat16 [16, 128, 128], P('tp'), may hold values from -0.5 to 0.5
- input_blocks: bfloat16 [16, 128, 128], P('tp'), may hold values from -0.5 to 0.5
- decay_param: float32 [2048], P('tp'), may hold values from 0 to 6
- out_proj: bfloat16 [2048, 2048], P('tp'), may hold values from -0.125 to 0.125
- first_gain: float32 [2048], replicated, may hold values from 0.1 to 1.9
- expert_gate: bfloat16 [4, 2048, 7168], P('ep', None, 'tp'), may hold values from -0.125 to 0.125
- expert_up: bfloat16 [4, 2048, 7168], P('ep', None, 'tp'), may hold values from -0.125 to 0.125
- expert_down: bfloat16 [4, 7168, 2048], P('ep', 'tp'), may hold values from -0.0625 to 0.0625
- routing: int32 [512, 2], P('ep'), may hold values from 0 to 3, all different within a row; in each aligned block of 128 rows (0 to 127, 128 to 255, ...) at most 128 rows name the same one
- route_weight: float32 [512, 2], P('ep'), may hold values from 0.1 to 1
- dense_gate: bfloat16 [2048, 2048], P(None, 'tp'), may hold values from -0.125 to 0.125
- dense_up: bfloat16 [2048, 2048], P(None, 'tp'), may hold values from -0.125 to 0.125
- dense_down: bfloat16 [2048, 2048], P('tp'), may hold values from -0.125 to 0.125
- mix_weight: bfloat16 [2048], replicated, may hold values from -0.125 to 0.125
- second_gain: float32 [2048], P('tp'), may hold values from 0.1 to 1.9
Outputs:
- layer_out: bfloat16 [512, 2048], P('ep', 'tp')
- new_state: float32 [512, 2048], P('ep', 'tp')
- new_conv: bfloat16 [512, 3, 2048], P('ep', None, 'tp')
Inputs may be any that keep to these rules, and one draw needn't show every extreme that they name: `routing`: each row names 2 different experts; in each aligned block of 128 rows (the rows of one index of ep) no expert is named by more than 128 rows, a bound that some expert reaches in some block.
All inputs are finite; a program needn't handle non-finite values.
Results may differ from a plain program's by a relative error of at most 0.013.
Values may be sent and summed in bfloat16 or wider, within the bound.
A program may use at most 64 MiB of HBM per device.

v0:
```python
import jax
import jax.numpy as jnp
from jax import lax
from jax.sharding import PartitionSpec as P

D = 2048
TOPK = 2


ALPHA = 8.0**0.25
RATE_SCALE = 8.0
NORM_EPS = 1e-05


def norm_rows(values, gain_vec):
    centre = values - jnp.mean(values, axis=-1, keepdims=True)
    spread = jnp.mean(centre * centre, axis=-1, keepdims=True)
    return centre * lax.rsqrt(spread + NORM_EPS) * gain_vec


def on_device(
    tokens,
    conv_state,
    rec_state,
    gate_proj,
    input_proj,
    conv_taps,
    decay_blocks,
    input_blocks,
    decay_param,
    out_proj,
    first_gain,
    expert_gate,
    expert_up,
    expert_down,
    routing,
    route_weight,
    dense_gate,
    dense_up,
    dense_down,
    mix_weight,
    second_gain,
):
    count_rows = tokens.shape[0]
    gated = jnp.dot(tokens, gate_proj, preferred_element_type=jnp.float32).astype(jnp.bfloat16)
    inputs = jnp.dot(tokens, input_proj, preferred_element_type=jnp.float32).astype(jnp.bfloat16)
    window = jnp.concatenate([conv_state, inputs[:, None, :]], axis=1)
    convolved = jnp.sum(
        window.astype(jnp.float32) * conv_taps.astype(jnp.float32)[None], axis=1
    ).astype(jnp.bfloat16)
    local_heads = decay_blocks.shape[0]
    heads_view = convolved.reshape(count_rows, local_heads, -1)
    recur_gate = jax.nn.sigmoid(
        jnp.einsum("bhi,hij->bhj", heads_view, decay_blocks, preferred_element_type=jnp.float32)
    ).reshape(count_rows, -1)
    input_gate = jax.nn.sigmoid(
        jnp.einsum("bhi,hij->bhj", heads_view, input_blocks, preferred_element_type=jnp.float32)
    ).reshape(count_rows, -1)
    log_decay = -RATE_SCALE * recur_gate * jax.nn.softplus(-decay_param)
    new_state = jnp.exp(log_decay) * rec_state + jnp.sqrt(
        -jnp.expm1(2.0 * log_decay)
    ) * input_gate * convolved.astype(jnp.float32)
    mixed_rows = (new_state * jax.nn.gelu(gated.astype(jnp.float32), approximate=True)).astype(
        jnp.bfloat16
    )
    partial_mix = jnp.dot(mixed_rows, out_proj, preferred_element_type=jnp.float32)
    mixed = lax.psum(partial_mix.astype(jnp.bfloat16), "tp").astype(jnp.float32)
    normed = norm_rows(ALPHA * tokens.astype(jnp.float32) + mixed, first_gain).astype(jnp.bfloat16)
    tp_index = lax.axis_index("tp")
    tp_count = lax.axis_size("tp")
    own_width = D // tp_count
    own_normed = lax.dynamic_slice_in_dim(normed, tp_index * own_width, own_width, 1)
    local_experts = expert_gate.shape[0]
    ep_count = lax.axis_size("ep")
    experts = local_experts * ep_count
    capacity = max(2, 2 * count_rows * TOPK // experts)
    flat_routes = routing.reshape(-1)
    labels = jnp.arange(experts, dtype=jnp.int32)
    onehot = (flat_routes[:, None] == labels[None, :]).astype(jnp.int32)
    earlier = jnp.cumsum(onehot, axis=0) - onehot
    slot_index = jnp.sum(earlier * onehot, axis=1)
    target = flat_routes * capacity + slot_index
    placed = (target[:, None] == jnp.arange(experts * capacity, dtype=jnp.int32)[None, :]).astype(
        jnp.bfloat16
    )
    token_slots = jnp.sum(placed.reshape(count_rows, TOPK, experts * capacity), axis=1)
    dispatch = jnp.dot(token_slots.T, normed, preferred_element_type=jnp.float32).astype(
        jnp.bfloat16
    )
    arrived = lax.all_to_all(
        dispatch.reshape(experts, capacity, D), "ep", split_axis=0, concat_axis=1, tiled=True
    )
    gate_val = jnp.einsum("erd,edf->erf", arrived, expert_gate, preferred_element_type=jnp.float32)
    up_val = jnp.einsum("erd,edf->erf", arrived, expert_up, preferred_element_type=jnp.float32)
    hidden = (jax.nn.silu(gate_val) * up_val).astype(jnp.bfloat16)
    partial_out = jnp.einsum(
        "erf,efd->erd", hidden, expert_down, preferred_element_type=jnp.float32
    )
    reduced = lax.psum_scatter(
        partial_out.astype(jnp.bfloat16), "tp", scatter_dimension=2, tiled=True
    )
    returned = lax.all_to_all(reduced, "ep", split_axis=1, concat_axis=0, tiled=True)
    returned = returned.reshape(experts * capacity, own_width)
    picked = jnp.dot(placed, returned, preferred_element_type=jnp.float32).reshape(
        count_rows, TOPK, own_width
    )
    routed_sum = jnp.sum(route_weight[:, :, None] * picked, axis=1)
    dense_g = jnp.dot(normed, dense_gate, preferred_element_type=jnp.float32)
    dense_u = jnp.dot(normed, dense_up, preferred_element_type=jnp.float32)
    dense_hidden = (jax.nn.silu(dense_g) * dense_u).astype(jnp.bfloat16)
    dense_part = jnp.dot(dense_hidden, dense_down, preferred_element_type=jnp.float32)
    dense_out = lax.psum_scatter(
        dense_part.astype(jnp.bfloat16), "tp", scatter_dimension=1, tiled=True
    ).astype(jnp.float32)
    mix = jax.nn.sigmoid(jnp.dot(normed, mix_weight, preferred_element_type=jnp.float32))
    combined = ALPHA * own_normed.astype(jnp.float32) + routed_sum + mix[:, None] * dense_out
    row_total, row_square = lax.psum(
        (jnp.sum(combined, axis=1), jnp.sum(combined * combined, axis=1)), "tp"
    )
    row_mean = row_total / D
    row_var = row_square / D - row_mean * row_mean
    layer_out = (
        (combined - row_mean[:, None]) * lax.rsqrt(row_var[:, None] + NORM_EPS) * second_gain
    ).astype(jnp.bfloat16)
    return (layer_out, new_state, window[:, 1:])


def solution(mesh):
    return jax.shard_map(
        on_device,
        mesh=mesh,
        in_specs=(
            P("ep", None),
            P("ep", None, "tp"),
            P("ep", "tp"),
            P(None, "tp"),
            P(None, "tp"),
            P(None, "tp"),
            P("tp", None, None),
            P("tp", None, None),
            P("tp"),
            P("tp", None),
            P(),
            P("ep", None, "tp"),
            P("ep", None, "tp"),
            P("ep", "tp", None),
            P("ep", None),
            P("ep", None),
            P(None, "tp"),
            P(None, "tp"),
            P("tp", None),
            P(),
            P("tp"),
        ),
        out_specs=(P("ep", "tp"), P("ep", "tp"), P("ep", None, "tp")),
        check_vma=False,
    )
```

profile of v0, /device:TPU:0, one launch (start us, length us, event | category | flops | bytes accessed | tf_op | source)
XLA Modules:
  0.0 208.7 jit_solution(3627572307212594813)
XLA Ops:
  7.3 0.8 convert_element_type.84
  8.0 1.8 fusion.23
  9.8 1.0 multiply_reduce_fusion.1
  10.8 1.1 fusion.20
  11.9 0.1 copy.91
  12.0 0.2 fusion.17
  12.3 0.1 copy.94
  12.4 0.1 multiply_add_fusion.1
  12.6 1.6 convolution_convert_fusion.2
  14.2 0.0 reduce-scatter.3.cloned.1.call-start
  14.3 0.1 copy.95
  14.4 0.1 eq.65
  14.5 0.1 eq.61
  14.7 1.2 reduce-window.6
  15.9 0.1 slice.12
  16.0 0.1 copy.97
  16.1 0.1 copy.98
  16.2 0.1 add_bitcast_fusion
  16.3 0.1 reduce_sum.81
  16.5 0.1 copy.99
  16.6 0.1 fusion.34
  16.7 56.9 %all-reduce.3.cloned.1.call-done = bf16[128,2048]{1,0:T(8,128)(2,1)} async-done(((bf16[128,2048]{1,0:T(8,128)(2,1)}), bf16[128,2048]{1,0:T(8,128)(2,1)}) %all-reduce.3.cloned.1.call-update) | async-done | bytes 524304 | tf_op jit(solution)/shard_map/psum | solution.py:67
  73.6 1.4 fusion.30
  75.0 1.4 multiply_reduce_fusion
  76.4 0.3 multiply_convert_fusion.1
  76.7 0.7 convolution_convert_fusion
  77.4 27.3 %all_to_all.8 = bf16[4,128,2048]{2,1,0:T(8,128)(2,1)S(1)} all-to-all(bf16[4,128,2048]{2,1,0:T(8,128)(2,1)S(1)} %bitcast.100), channel_id=1, replica_groups=mesh['ep'=4,'tp'=8] {'ep'}, dimensions={0} | all-to-all | bytes 4194304 | tf_op jit(solution)/shard_map/all_to_all | solution.py:90
  104.7 1.3 copy-done.3
  106.0 3.6 %fusion.4 = f32[512,896]{1,0:T(8,128)} fusion(bf16[512,2048]{1,0:T(8,128)(2,1)S(1)} %bitcast.101, bf16[1,2048,896]{2,1,0:T(8,128)(2,1)S(1)} %copy-done.14), kind=kOutput, calls=%fused_computation.4 | convolution fusion | flops 1879048192 | bytes 7602176 | tf_op jit(solution)/shard_map/erd,edf->erf/dot_general | solution.py:93
  109.6 10.2 %fusion.9 = bf16[1,512,2048]{2,1,0:T(8,128)(2,1)} fusion(bf16[1,896,2048]{2,1,0:T(8,128)(2,1)} %param.34, f32[512,896]{1,0:T(8,128)} %fusion.4, bf16[512,2048]{1,0:T(8,128)(2,1)} %bitcast.102, bf16[1,2048,896]{2,1,0:T(8,128)(2,1)} %param.33), kind=kOutput, calls=%fused_computation.8 | convolution fusion | flops 3761897472 | bytes 13369344 | tf_op jit(solution)/shard_map/erf,efd->erd/dot_general | solution.py:96
  119.8 0.0 reduce-scatter.5.cloned.1.call-start
  119.9 1.6 fusion.73
  121.5 2.8 %convolution_convert_fusion.1 = bf16[128,2048]{1,0:T(8,128)(2,1)} fusion(bf16[256,2048]{1,0:T(8,128)(2,1)S(1)} %copy-done.5, bf16[128,2048]{1,0:T(8,128)(2,1)S(1)} %multiply_convert_fusion.1, bf16[2048,256]{1,0:T(8,128)(2,1)} %param.38, f32[128,256]{1,0:T(8,128)S(1)} %fusion.73), kind=kOutput, calls=%fused_computation.9 | convolution fusion | flops 268894208 | bytes 3276800 | tf_op jit(solution)/shard_map/dot_general | solution.py:111
  124.4 0.7 fusion.38
  125.1 29.4 %reduce-scatter.3.cloned.1.call-done = bf16[1,512,256]{2,1,0:T(8,128)(2,1)} async-done(((bf16[1,512,2048]{2,1,0:T(8,128)(2,1)}), bf16[1,512,256]{2,1,0:T(8,128)(2,1)}) %reduce-scatter.3.cloned.1.call-update) | async-done | bytes 262160 | tf_op jit(solution)/shard_map/reduce_scatter | solution.py:99
  154.6 1.4 copy.120
  155.9 0.5 broadcast.115
  156.4 2.2 %reduce.1 = bf16[512,256]{1,0:T(8,128)(2,1)S(1)} reduce(bf16[512,1,256]{2,1,0:T(2,128)(2,1)S(1)} %bitcast.103, bf16[]{:T(256)} %broadcast.115), dimensions={1}, to_apply=%bitcast.99.reduce_sub_computation | reduce | bytes 524290
  158.7 0.8 reshape.150
  159.4 3.7 %all-to-all-start.1 = ((bf16[4,2,16384]{2,1,0:T(2,128)(2,1)}), bf16[4,2,16384]{2,1,0:T(2,128)(2,1)S(1)}, u32[]{:S(2)}, u32[]{:S(2)}) async-start(bf16[4,2,16384]{2,1,0:T(2,128)(2,1)} %reshape.150), calls=%async_computation.2 | async-start | bytes 524288 | tf_op jit(solution)/shard_map/all_to_all | solution.py:102
  163.1 0.2 fusion.27
  163.3 5.1 %all-to-all-done.1 = bf16[4,2,16384]{2,1,0:T(2,128)(2,1)S(1)} async-done(((bf16[4,2,16384]{2,1,0:T(2,128)(2,1)}), bf16[4,2,16384]{2,1,0:T(2,128)(2,1)S(1)}, u32[]{:S(2)}, u32[]{:S(2)}) %all-to-all-start.1) | async-done | bytes 262176 | tf_op jit(solution)/shard_map/all_to_all | solution.py:102
  168.4 0.3 reshape.151
  168.7 0.3 fusion.14
  169.0 17.6 %reduce-scatter.5.cloned.1.call-done = bf16[128,256]{1,0:T(8,128)(2,1)} async-done(((bf16[128,2048]{1,0:T(8,128)(2,1)}), bf16[128,256]{1,0:T(8,128)(2,1)}) %reduce-scatter.5.cloned.1.call-update) | async-done | bytes 65552 | tf_op jit(solution)/shard_map/reduce_scatter | solution.py:112
  186.7 1.0 fusion.72
  187.7 13.7 %all-reduce = (f32[128]{0:T(128)S(1)}, f32[128]{0:T(128)S(1)}) all-reduce(f32[128]{0:T(128)S(1)} %get-tuple-element.4, f32[128]{0:T(128)S(1)} %get-tuple-element.3), channel_id=1, replica_groups=mesh['ep'=4,'tp'=8] {'tp'}, use_global_device_ids=true, to_apply=%region_14.15 | all-reduce | flops 256 | bytes 2048 | tf_op jit(solution)/shard_map/psum | solution.py:117
  201.4 0.7 multiply_convert_fusion.2
  (47 shorter events, 0.3 us)
Async XLA Ops:
  7.2 5.4 %copy-start = (bf16[256,2048]{1,0:T(8,128)(2,1)S(1)}, bf16[256,2048]{1,0:T(8,128)(2,1)}, u32[]{:S(2)}) copy-start(bf16[256,2048]{1,0:T(8,128)(2,1)} %param.30) | copy-start | bytes 3145732
  7.2 4.8 %copy-start.15 = (bf16[2,128,128]{2,1,0:T(8,128)(2,1)S(1)}, bf16[2,128,128]{2,1,0:T(8,128)(2,1)}, u32[]{:S(2)}) copy-start(bf16[2,128,128]{2,1,0:T(8,128)(2,1)} %param.28) | copy-start | bytes 196612
  7.2 5.2 %copy-start.13 = (f32[256]{0:T(256)S(1)}, f32[256]{0:T(256)}, u32[]{:S(2)}) copy-start(f32[256]{0:T(256)} %param.29) | copy-start | bytes 3076
  7.2 5.2 %copy-start.8 = (f32[128,256]{1,0:T(8,128)S(1)}, f32[128,256]{1,0:T(8,128)}, u32[]{:S(2)}) copy-start(f32[128,256]{1,0:T(8,128)} %param.23) | copy-start | bytes 393220
  7.2 66.4 %all-reduce.3.cloned.1.call-start = ((), (), s32[]{:S(2)}) async-start(), calls=%async_computation.4 | async-start | bytes 1048576 | tf_op jit(solution)/shard_map/psum | solution.py:67
  8.0 4.5 %copy-start.1 = (bf16[128,2048]{1,0:T(8,128)(2,1)S(1)}, bf16[128,2048]{1,0:T(8,128)(2,1)}, u32[]{:S(2)}) copy-start(bf16[128,2048]{1,0:T(8,128)(2,1)} %param.21) | copy-start | bytes 1572868
  8.0 4.5 %copy-start.4 = (bf16[2048,256]{1,0:T(8,128)(2,1)S(1)}, bf16[2048,256]{1,0:T(8,128)(2,1)}, u32[]{:S(2)}) copy-start(bf16[2048,256]{1,0:T(8,128)(2,1)} %param.24) | copy-start | bytes 3145732
  12.4 1.9 copy-start.10
  12.6 4.0 %copy-start.7 = (f32[128,256]{1,0:T(8,128)}, f32[128,256]{1,0:T(8,128)S(1)}, u32[]{:S(2)}) copy-start(f32[128,256]{1,0:T(8,128)S(1)} %multiply_add_fusion.1) | copy-start | bytes 393220
  14.2 62.2 %copy-start.9 = (f32[2048]{0:T(1024)S(1)}, f32[2048]{0:T(1024)}, u32[]{:S(2)}) copy-start(f32[2048]{0:T(1024)} %param.31) | copy-start | bytes 24580
  14.2 140.3 %reduce-scatter.3.cloned.1.call-start = ((), (), s32[]{:S(2)}) async-start(), calls=%async_computation.5 | async-start | bytes 2359296 | tf_op jit(solution)/shard_map/reduce_scatter | solution.py:99
  73.6 2.8 %copy-start.2 = (bf16[128,2048]{1,0:T(8,128)(2,1)S(1)}, bf16[128,2048]{1,0:T(8,128)(2,1)}, u32[]{:S(2)}) copy-start(bf16[128,2048]{1,0:T(8,128)(2,1)} %all-reduce.3.cloned.1.call-done) | copy-start | bytes 1572868
  77.4 28.6 %copy-start.14 = (bf16[1,2048,896]{2,1,0:T(8,128)(2,1)S(1)}, bf16[1,2048,896]{2,1,0:T(8,128)(2,1)}, u32[]{:S(2)}) copy-start(bf16[1,2048,896]{2,1,0:T(8,128)(2,1)} %param.32) | copy-start | bytes 11010052
  104.7 1.3 copy-start.3
  119.8 1.7 copy-start.5
  119.8 66.8 %reduce-scatter.5.cloned.1.call-start = ((), (), s32[]{:S(2)}) async-start(), calls=%async_computation.6 | async-start | bytes 589824 | tf_op jit(solution)/shard_map/reduce_scatter | solution.py:112
  121.5 2.9 %copy-start.11 = (bf16[2048]{0:T(1024)(128)(2,1)S(1)}, bf16[2048]{0:T(1024)(128)(2,1)}, u32[]{:S(2)}) copy-start(bf16[2048]{0:T(1024)(128)(2,1)} %param.40) | copy-start | bytes 12292
  121.5 2.9 %copy-start.6 = (bf16[128,3,256]{2,0,1:T(8,128)(2,1)S(1)}, bf16[128,3,256]{2,0,1:T(8,128)(2,1)}, u32[]{:S(2)}) copy-start(bf16[128,3,256]{2,0,1:T(8,128)(2,1)} %param.22) | copy-start | bytes 589828
  124.4 44.3 %copy-start.16 = (f32[128,2]{0,1:T(2,128)S(1)}, f32[128,2]{0,1:T(2,128)}, u32[]{:S(2)}) copy-start(f32[128,2]{0,1:T(2,128)} %param.36) | copy-start | bytes 3076
  156.4 45.0 %copy-start.12 = (f32[256]{0:T(256)S(1)}, f32[256]{0:T(256)}, u32[]{:S(2)}) copy-start(f32[256]{0:T(256)} %param.41) | copy-start | bytes 3076
  159.4 9.0 %all-to-all-start.1 = ((bf16[4,2,16384]{2,1,0:T(2,128)(2,1)}), bf16[4,2,16384]{2,1,0:T(2,128)(2,1)S(1)}, u32[]{:S(2)}, u32[]{:S(2)}) async-start(bf16[4,2,16384]{2,1,0:T(2,128)(2,1)} %reshape.150), calls=%async_computation.2 | async-start | bytes 524288 | tf_op jit(solution)/shard_map/all_to_all | solution.py:102
Sparse Core Ops, SparseCore 0:
  14.3 59.2 all-reduce.2
  119.9 34.5 reduce-scatter.2
  156.8 29.8 reduce-scatter.4
where the time goes:
time: 209 us
  waiting for transfers between devices  109 us (52%)
  blocking collectives  41 us (20%)
  matrix products  24.2 us (12%)
  between operations  14.1 us (7%)
  other arithmetic  11.1 us (5%)
  local copies, waits for them, and re-layouts  5.33 us (3%)
  starting transfers between devices  3.79 us (2%)
    psum x1, waiting for transfers between devices, on_device(): mixed = lax.psum(partial_mix.astype(jnp.bfloat16), 'tp').astype(jnp.float32)  56.9 us
    reduce_scatter x1, waiting for transfers between devices, on_device(): lax.psum_scatter(partial_out.astype(jnp.bfloat16), 'tp', scatter_dimensio...  29.4 us
    all_to_all x1, blocking collectives, on_device(): lax.all_to_all(dispatch.reshape(experts, capacity, D), 'ep', split_axis=0...  27.3 us
    reduce_scatter x1, waiting for transfers between devices, on_device(): lax.psum_scatter(dense_part.astype(jnp.bfloat16), 'tp', scatter_dimension...  17.6 us
    psum x1, blocking collectives, on_device(): lax.psum((jnp.sum(combined, axis=1), jnp.sum(combined * combined, axis=1)...  13.7 us
    dot_general x1, matrix products, on_device(): jnp.einsum('erf,efd->erd', hidden, expert_down, preferred_element_type=jn...  10.2 us
    all_to_all x1, waiting for transfers between devices, on_device(): lax.all_to_all(reduced, 'ep', split_axis=1, concat_axis=0, tiled=True)  5.13 us
  transfers between devices with their start and end apart: 4, of which 4 were waited for; matrix products, arithmetic and copies ran while one was open for 6% of the time, Pallas kernels for 0%

commit v1 on v0

--- a/solution.py
+++ b/solution.py
@@ -1,6 +1,10 @@
+import functools
+
 import jax
 import jax.numpy as jnp
 from jax import lax
+from jax.experimental import pallas as pl
+from jax.experimental.pallas import tpu as pltpu
 from jax.sharding import PartitionSpec as P
 
 D = 2048
@@ -18,7 +22,7 @@
     return centre * lax.rsqrt(spread + NORM_EPS) * gain_vec
 
 
-def on_device(
+def on_device_slots(
     tokens,
     conv_state,
     rec_state,
@@ -125,6 +129,438 @@
     return (layer_out, new_state, window[:, 1:])
 
 
+MESH = pl.DeviceIdType.MESH
+
+
+def xor(left, right, count):
+    total, bit = 0, 1
+    while bit < count:
+        lbit, rbit = (left // bit) % 2, (right // bit) % 2
+        total = total + bit * (lbit + rbit - 2 * lbit * rbit)
+        bit *= 2
+    return total
+
+
+def block_kernel(
+    n_ep,
+    n_tp,
+    tokens_hbm,
+    conv_ref,
+    state_ref,
+    gproj_hbm,
+    iproj_hbm,
+    taps_ref,
+    dblk_ref,
+    iblk_ref,
+    dparam_ref,
+    oproj_hbm,
+    fgain_ref,
+    eg_hbm,
+    eu_hbm,
+    ed_hbm,
+    routing_ref,
+    rweight_ref,
+    dg_hbm,
+    du_hbm,
+    dd_hbm,
+    mixw_ref,
+    sgain_ref,
+    out_ref,
+    nstate_ref,
+    nconv_ref,
+    tok,
+    gproj,
+    iproj,
+    oproj,
+    eg,
+    eu,
+    ed,
+    dg,
+    du,
+    dd,
+    pmix,
+    pmix_in,
+    smix,
+    smix_in,
+    xall,
+    hid,
+    dhid,
+    wtab,
+    part,
+    part_in,
+    psum,
+    ret_in,
+    zout,
+    zin,
+    oout,
+    oin,
+    wsem,
+    bpair,
+    bz_s,
+    bz_r,
+    agz_s,
+    agz_r,
+    age_s,
+    age_r,
+    sib_s,
+    sib_r,
+    rp_s,
+    rp_r,
+    re_s,
+    re_r,
+    rz_s,
+    rz_r,
+    o_s,
+    o_r,
+):
+    f32, bf16 = jnp.float32, jnp.bfloat16
+    e, t = lax.axis_index("ep"), lax.axis_index("tp")
+    n_z = n_tp // 2
+    c, k = t % 2, t // 2
+    other = 1 - c
+    sibling = 2 * k + other
+    rr, width = tok.shape[1], tok.shape[2]
+    rows = n_tp * rr
+    wide = min(512, width)
+
+    loads = [
+        pltpu.make_async_copy(a, b, wsem.at[i])
+        for i, (a, b) in enumerate(
+            [
+                (tokens_hbm, tok),
+                (iproj_hbm, iproj),
+                (gproj_hbm, gproj),
+                (oproj_hbm, oproj),
+                (dg_hbm, dg),
+                (du_hbm, du),
+                (dd_hbm, dd),
+                (eg_hbm, eg),
+                (eu_hbm, eu),
+                (ed_hbm, ed),
+            ]
+        )
+    ]
+    for load in loads:
+        load.start()
+
+    barrier = pltpu.get_barrier_semaphore()
+    for d in range(1, n_tp):
+        pl.semaphore_signal(barrier, inc=1, device_id=(e, xor(t, d, n_tp)), device_id_type=MESH)
+    for d in range(1, n_ep):
+        pl.semaphore_signal(barrier, inc=1, device_id=(xor(e, d, n_ep), t), device_id_type=MESH)
+
+    def remote(src, dst, send, recv, ep, tp):
+        return pltpu.make_async_remote_copy(
+            src_ref=src, dst_ref=dst, send_sem=send, recv_sem=recv,
+            device_id=(ep, tp), device_id_type=MESH,
+        )
+
+    route, rweight = routing_ref[...], rweight_ref[...]
+    for s in range(n_ep):
+        col = jnp.zeros((rows, 1), f32)
+        for j in range(TOPK):
+            col = col + jnp.where(route[:, j : j + 1] == s, rweight[:, j : j + 1], 0.0)
+        wtab[s] = jnp.broadcast_to(col, (rows, 128)).reshape(n_tp, rr, 128)
+
+    loads[0].wait()
+    loads[1].wait()
+    tokens = tok[...].reshape(rows, width)
+    inputs = jnp.dot(tokens, iproj[...], preferred_element_type=f32).astype(bf16)
+    taps = taps_ref[...].astype(f32)
+    conv = inputs.astype(f32) * taps[3:4]
+    for j in range(3):
+        conv = conv + conv_ref[j].astype(f32) * taps[j : j + 1]
+    nconv_ref[0] = conv_ref[1]
+    nconv_ref[1] = conv_ref[2]
+    nconv_ref[2] = inputs
+    conv = conv.astype(bf16)
+    heads, blk = dblk_ref.shape[0], dblk_ref.shape[1]
+
+    def by_head(ref):
+        parts = [
+            jnp.dot(conv[:, h * blk : (h + 1) * blk], ref[h], preferred_element_type=f32)
+            for h in range(heads)
+        ]
+        return jax.nn.sigmoid(jnp.concatenate(parts, axis=1))
+
+    recur_gate, input_gate = by_head(dblk_ref), by_head(iblk_ref)
+    neg = -dparam_ref[...]
+    soft = jnp.maximum(neg, 0.0) + jnp.log1p(jnp.exp(-jnp.abs(neg)))
+    log_decay = -RATE_SCALE * recur_gate * soft
+    decay = jnp.exp(log_decay)
+    new_state = decay * state_ref[...] + jnp.sqrt(
+        -jnp.tanh(log_decay) * (decay * decay + 1.0)
+    ) * input_gate * conv.astype(f32)
+    nstate_ref[...] = new_state
+    loads[2].wait()
+    gated = jnp.dot(tokens, gproj[...], preferred_element_type=f32).astype(bf16).astype(f32)
+    mixed = (new_state * jax.nn.gelu(gated, approximate=True)).astype(bf16)
+    loads[3].wait()
+    for n0 in range(0, width, wide):
+        val = jnp.dot(mixed, oproj[:, n0 : n0 + wide], preferred_element_type=f32).astype(bf16)
+        for j in range(n_tp):
+            pmix[j % 2, j // 2, :, n0 : n0 + wide] = val[j * rr : (j + 1) * rr]
+    pl.semaphore_wait(barrier, n_tp - 1 + n_ep - 1)
+
+    copy = remote(pmix.at[other], pmix_in, bpair.at[0], bpair.at[1], e, sibling)
+    copy.start()
+    copy.wait_recv()
+    zcopies = []
+    for d in range(1, n_z):
+        kk = xor(k, d, n_z)
+        smix[d] = (pmix[c, kk].astype(f32) + pmix_in[kk].astype(f32)).astype(bf16)
+        zc = remote(smix.at[d], smix_in.at[d], bz_s.at[d], bz_r.at[d], e, 2 * kk + c)
+        zc.start()
+        zcopies.append(zc)
+    mix_rows = pmix[c, k].astype(f32) + pmix_in[k].astype(f32)
+    mix_rows = mix_rows + ALPHA * tok[t].astype(f32)
+    for d in range(1, n_z):
+        zcopies[d - 1].wait_recv()
+        mix_rows = mix_rows + smix_in[d].astype(f32)
+    normed = norm_rows(mix_rows, fgain_ref[...]).astype(bf16)
+    xall[e, c, k] = normed
+
+    def block(dge, dk):
+        return xall.at[xor(e, dge, n_ep), c, xor(k, dk, n_z)]
+
+    agz, age, sib = [], {}, {}
+    own = xall.at[e, c, k]
+    for d in range(1, n_z):
+        zc = remote(own, own, agz_s.at[d], agz_r.at[d], e, 2 * xor(k, d, n_z) + c)
+        zc.start()
+        agz.append(zc)
+
+    def to_ep(dge, dk):
+        src = xall.at[e, c, xor(k, dk, n_z)]
+        ec = remote(src, src, age_s.at[dge, dk], age_r.at[dge, dk], xor(e, dge, n_ep), t)
+        ec.start()
+        age[dge, dk] = ec
+
+    single = [d for d in range(1, n_ep) if d & (d - 1) == 0]
+    double = [d for d in range(1, n_ep) if d & (d - 1)]
+    for dge in single:
+        to_ep(dge, 0)
+    for d in range(1, n_z):
+        agz[d - 1].wait_recv()
+        for dge in single:
+            to_ep(dge, d)
+    for d in range(n_z):
+        for dge in double:
+            to_ep(dge, d)
+
+    def to_sibling(dge):
+        src = xall.at[xor(e, dge, n_ep), c]
+        return remote(src, src, sib_s.at[dge], sib_r.at[dge], e, sibling)
+
+    def from_ep(dge):
+        for dk in range(n_z):
+            dst = xall.at[xor(e, dge, n_ep), c, xor(k, dk, n_z)]
+            remote(dst, dst, age_s.at[dge, dk], age_r.at[dge, dk], xor(e, dge, n_ep), t).wait_recv()
+
+    to_sibling(0).start()
+    to_sibling(0).wait_recv()
+
+    ff = eg.shape[1]
+    rows_own = xall[e].reshape(rows, width)
+    for i in (4, 5):
+        loads[i].wait()
+    dhid[...] = (
+        jax.nn.silu(jnp.dot(rows_own, dg[...], preferred_element_type=f32))
+        * jnp.dot(rows_own, du[...], preferred_element_type=f32)
+    ).astype(bf16)
+    mix = jax.nn.sigmoid(
+        jnp.sum(rows_own.astype(f32) * mixw_ref[...].astype(f32), axis=1, keepdims=True)
+    )
+    for i in (6, 7, 8, 9):
+        loads[i].wait()
+
+    def hidden(g):
+        x = xall[g].reshape(rows, width)
+        for f0 in range(0, ff, 256):
+            f1 = min(ff, f0 + 256)
+            gate_val = jnp.dot(x, eg[:, f0:f1], preferred_element_type=f32)
+            up_val = jnp.dot(x, eu[:, f0:f1], preferred_element_type=f32)
+            hid[:, f0:f1] = (jax.nn.silu(gate_val) * up_val).astype(bf16)
+
+    def to_pair(dge):
+        return remote(
+            part.at[dge, other], part_in.at[dge], rp_s.at[dge], rp_r.at[dge], e, sibling
+        )
+
+    def to_owner(dge):
+        return remote(
+            psum.at[dge], ret_in.at[dge], re_s.at[dge], re_r.at[dge], xor(e, dge, n_ep), t
+        )
+
+    hidden(e)
+    weights = jnp.concatenate(
+        [wtab[e, 2 * kk + cc][:, :1] for cc in range(2) for kk in range(n_z)], axis=0
+    )
+    for n0 in range(0, width, wide):
+        val = weights * jnp.dot(hid[...], ed[:, n0 : n0 + wide], preferred_element_type=f32)
+        val = val + mix * jnp.dot(dhid[...], dd[:, n0 : n0 + wide], preferred_element_type=f32)
+        part[0, :, :, :, n0 : n0 + wide] = val.astype(bf16).reshape(2, n_z, rr, wide)
+    to_pair(0).start()
+
+    def finish(dge):
+        to_pair(dge).wait_recv()
+        for kk in range(n_z):
+            psum[dge, kk] = (
+                part[dge, c, kk].astype(f32) + part_in[dge, kk].astype(f32)
+            ).astype(bf16)
+        to_owner(dge).start()
+
+    def step(dge, carry):
+        from_ep(dge)
+        to_sibling(dge).start()
+        to_sibling(dge).wait_recv()
+        hidden(xor(e, dge, n_ep))
+        for n0 in range(0, width, wide):
+            val = jnp.dot(hid[...], ed[:, n0 : n0 + wide], preferred_element_type=f32)
+            part[dge, :, :, :, n0 : n0 + wide] = val.astype(bf16).reshape(2, n_z, rr, wide)
+        to_pair(dge).start()
+        finish(dge)
+        return carry
+
+    lax.fori_loop(1, n_ep, step, 0)
+
+    to_pair(0).wait_recv()
+    for dge in range(1, n_ep):
+        to_owner(dge).wait_recv()
+
+    def combine(kk):
+        total = part[0, c, kk].astype(f32) + part_in[0, kk].astype(f32)
+        for dge in range(1, n_ep):
+            weight = wtab[xor(e, dge, n_ep), 2 * kk + c][:, :1]
+            total = total + weight * ret_in[dge, kk].astype(f32)
+        return total
+
+    zcopies2 = []
+    for d in range(1, n_z):
+        kk = xor(k, d, n_z)
+        zout[d] = combine(kk).astype(bf16)
+        zc = remote(zout.at[d], zin.at[d], rz_s.at[d], rz_r.at[d], e, 2 * kk + c)
+        zc.start()
+        zcopies2.append(zc)
+    total = combine(k) + ALPHA * xall[e, c, k].astype(f32)
+    for d in range(1, n_z):
+        zcopies2[d - 1].wait_recv()
+        total = total + zin[d].astype(f32)
+    final = norm_rows(total, 1.0)
+    cols = width // n_tp
+    for j in range(n_tp):
+        oout[j] = final[:, j * cols : (j + 1) * cols]
+    ocopies = []
+    for d in range(1, n_tp):
+        peer = xor(t, d, n_tp)
+        oc = remote(oout.at[peer], oin.at[t], o_s.at[d], o_r.at[d], e, peer)
+        oc.start()
+        ocopies.append(oc)
+    oin[t] = oout[t]
+    for d in range(1, n_tp):
+        peer = xor(t, d, n_tp)
+        remote(oout.at[peer], oin.at[peer], o_s.at[d], o_r.at[d], e, peer).wait_recv()
+    out_ref[...] = (oin[...].reshape(rows, cols) * sgain_ref[...]).astype(bf16)
+
+    copy.wait_send()
+    for group in (zcopies, agz, zcopies2, ocopies):
+        for each in group:
+            each.wait_send()
+    for each in age.values():
+        each.wait_send()
+    for dge in range(n_ep):
+        to_sibling(dge).wait_send()
+        to_pair(dge).wait_send()
+        if dge:
+            to_owner(dge).wait_send()
+
+
+def on_device(*args):
+    tokens, routing, expert_gate = args[0], args[14], args[11]
+    rows, width = tokens.shape
+    n_ep, n_tp = lax.axis_size("ep"), lax.axis_size("tp")
+    experts = expert_gate.shape[0] * n_ep
+    capacity = max(2, 2 * rows * TOPK // experts)
+    if capacity < rows or expert_gate.shape[0] != 1 or n_ep & (n_ep - 1) or n_tp & (n_tp - 1):
+        return on_device_slots(*args)
+    rr, n_z = rows // n_tp, n_tp // 2
+    own, ff = args[3].shape[1], expert_gate.shape[2]
+    bf16, f32 = jnp.bfloat16, jnp.float32
+    operands = list(args)
+    operands[0] = tokens.reshape(n_tp, rr, width)
+    operands[1] = jnp.transpose(args[1], (1, 0, 2))
+    for i in (8, 10, 19, 20):
+        operands[i] = args[i].reshape(1, -1)
+    for i in (11, 12, 13):
+        operands[i] = args[i][0]
+    in_hbm = (0, 3, 4, 9, 11, 12, 13, 16, 17, 18)
+    vmem = pl.BlockSpec(memory_space=pltpu.VMEM)
+    dma = pltpu.SemaphoreType.DMA
+    layer_out, new_state, new_conv = pl.pallas_call(
+        functools.partial(block_kernel, n_ep, n_tp),
+        out_shape=(
+            jax.ShapeDtypeStruct((rows, own), bf16),
+            jax.ShapeDtypeStruct((rows, own), f32),
+            jax.ShapeDtypeStruct((3, rows, own), bf16),
+        ),
+        in_specs=[
+            pl.BlockSpec(memory_space=pl.ANY) if i in in_hbm else vmem
+            for i in range(len(operands))
+        ],
+        out_specs=(vmem, vmem, vmem),
+        scratch_shapes=[
+            pltpu.VMEM((n_tp, rr, width), bf16),
+            pltpu.VMEM((width, own), bf16),
+            pltpu.VMEM((width, own), bf16),
+            pltpu.VMEM((own, width), bf16),
+            pltpu.VMEM((width, ff), bf16),
+            pltpu.VMEM((width, ff), bf16),
+            pltpu.VMEM((ff, width), bf16),
+            pltpu.VMEM(args[16].shape, bf16),
+            pltpu.VMEM(args[17].shape, bf16),
+            pltpu.VMEM(args[18].shape, bf16),
+            pltpu.VMEM((2, n_z, rr, width), bf16),
+            pltpu.VMEM((n_z, rr, width), bf16),
+            pltpu.VMEM((n_z, rr, width), bf16),
+            pltpu.VMEM((n_z, rr, width), bf16),
+            pltpu.VMEM((n_ep, 2, n_z, rr, width), bf16),
+            pltpu.VMEM((rows, ff), bf16),
+            pltpu.VMEM((rows, args[16].shape[1]), bf16),
+            pltpu.VMEM((n_ep, n_tp, rr, 128), f32),
+            pltpu.VMEM((n_ep, 2, n_z, rr, width), bf16),
+            pltpu.VMEM((n_ep, n_z, rr, width), bf16),
+            pltpu.VMEM((n_ep, n_z, rr, width), bf16),
+            pltpu.VMEM((n_ep, n_z, rr, width), bf16),
+            pltpu.VMEM((n_z, rr, width), bf16),
+            pltpu.VMEM((n_z, rr, width), bf16),
+            pltpu.VMEM((n_tp, rr, width // n_tp), f32),
+            pltpu.VMEM((n_tp, rr, width // n_tp), f32),
+            dma((len(in_hbm),)),
+            dma((2,)),
+            dma((n_z,)),
+            dma((n_z,)),
+            dma((n_z,)),
+            dma((n_z,)),
+            dma((n_ep, n_z)),
+            dma((n_ep, n_z)),
+            dma((n_ep,)),
+            dma((n_ep,)),
+            dma((n_ep,)),
+            dma((n_ep,)),
+            dma((n_ep,)),
+            dma((n_ep,)),
+            dma((n_z,)),
+            dma((n_z,)),
+            dma((n_tp,)),
+            dma((n_tp,)),
+        ],
+        compiler_params=pltpu.CompilerParams(
+            collective_id=0, has_side_effects=True, vmem_limit_bytes=56 * 2**20
+        ),
+    )(*operands)
+    return layer_out, new_state, jnp.transpose(new_conv, (1, 0, 2))
+
+
 def solution(mesh):
     return jax.shard_map(
         on_device,

time: 209 us -> 72.8 us (0.35)
  waiting for transfers between devices: 109 us -> 0 us
  Pallas kernels: 0 us -> 63.1 us
  blocking collectives: 41 us -> 0 us
  matrix products: 24.2 us -> 0 us
  between operations: 14.1 us -> 0.64 us
  other arithmetic: 11.1 us -> 0 us
  starting transfers between devices: 3.79 us -> 0 us
  local copies, waits for them, and re-layouts: 5.33 us -> 8.77 us
    pallas_call x0 -> x1, Pallas kernels: none -> 63.1 us  [on_device(): pl.pallas_call(functools.partial(block_kernel, n_ep, n_tp), out_shape=(ja...]
    psum x1 -> x0, waiting for transfers between devices: 56.9 us -> none  [on_device(): mixed = lax.psum(partial_mix.astype(jnp.bfloat16), 'tp').astype(jnp.float32)]
    reduce_scatter x2 -> x0, waiting for transfers between devices: 47.1 us -> none  [the longest x1 29.4 us: on_device(): lax.psum_scatter(partial_out.astype(jnp.bfloat16), 'tp', scatter_dimensio...]
    all_to_all x1 -> x0, blocking collectives: 27.3 us -> none  [on_device(): lax.all_to_all(dispatch.reshape(experts, capacity, D), 'ep', split_axis=0...]
    dot_general x11 -> x0, matrix products: 24.2 us -> none  [the longest x1 10.2 us: on_device(): jnp.einsum('erf,efd->erd', hidden, expert_down, preferred_element_type=jn...]
    psum x1 -> x0, blocking collectives: 13.7 us -> none  [on_device(): lax.psum((jnp.sum(combined, axis=1), jnp.sum(combined * combined, axis=1)...]
    all_to_all x1 -> x0, waiting for transfers between devices: 5.13 us -> none  [on_device(): lax.all_to_all(reduced, 'ep', split_axis=1, concat_axis=0, tiled=True)]
    reduce_sum x6 -> x0, other arithmetic: 4.89 us -> none  [the longest x1 1.37 us: norm_rows(): centre = values - jnp.mean(values, axis=-1, keepdims=True)]
  transfers between devices with their start and end apart: 4 -> 0, of which waited for: 4 -> 0; matrix products, arithmetic and copies ran while one was open for 6% -> 0% of each run, Pallas kernels for 0% -> 0%
where the time goes in v1:
time: 72.8 us; the launch traced here: 72.5 us
  Pallas kernels  63.1 us (87%)
  local copies, waits for them, and re-layouts  8.77 us (12%)
    pallas_call x1, Pallas kernels, on_device(): pl.pallas_call(functools.partial(block_kernel, n_ep, n_tp), out_shape=(ja...  63.1 us
    unnamed x5, local copies, waits for them, and re-layouts  7.48 us

profile of v1, /device:TPU:0, one launch (start us, length us, event | category | flops | bytes accessed | tf_op | source)
XLA Modules:
  0.0 72.5 jit_solution(8493566300664858550)
XLA Ops:
  0.6 1.3 %reshape.24.mixw_ref = bf16[1,2048]{1,0:T(2,128)(2,1)} reshape(bf16[2048]{0:T(1024)(128)(2,1)} %param.40) | data formatting | bytes 8192 | tf_op jit(solution)/shard_map/reshape | solution.py:493
  1.9 1.4 %copy.24.routing_ref = s32[128,2]{1,0:T(8,128)} copy(s32[128,2]{0,1:T(2,128)} %param.35) | data formatting | bytes 2048 | tf_op args[14]
  3.3 1.4 %copy.25.rweight_ref = f32[128,2]{1,0:T(8,128)} copy(f32[128,2]{0,1:T(2,128)} %param.36) | data formatting | bytes 2048 | tf_op args[15]
  4.7 63.1 %shard_map.220 = (bf16[128,256]{1,0:T(8,128)(2,1)}, f32[128,256]{1,0:T(8,128)}, bf16[3,128,256]{2,1,0:T(8,128)(2,1)}) custom-call(bf16[8,16,2048]{2,1,0:T(8,128)(2,1)} %bitcast.12, bf16[3,128,256]{2,1,0:T(8,128)(2,1)} %bitcast.13, f32[128,256]{1,0:T(8,128)} %state_ref.1, bf16[2048,256]{1,0:T(8,128)(2,1)} %gproj_hbm.1, bf16[2048,256]{1,0:T(8,128)(2,1)} %iproj_hbm.1, ...), custom_call_target="tpu_custom_call" | custom-call | tf_op jit(solution)/shard_map/pallas_call | solution.py:499
  67.8 1.5 %copy.29 = bf16[128,256]{1,0:T(8,128)(2,1)} copy(bf16[128,256]{1,0:T(8,128)(2,1)} %get-tuple-element.12) | data formatting | bytes 131072
  69.3 1.6 %copy.30 = f32[128,256]{1,0:T(8,128)} copy(f32[128,256]{1,0:T(8,128)} %get-tuple-element.13) | data formatting | bytes 262144
  70.9 1.6 %copy.31 = bf16[128,3,256]{2,0,1:T(8,128)(2,1)} copy(bf16[128,3,256]{2,0,1:T(8,128)(2,1)} %bitcast.14) | data formatting | bytes 393216

commit v2 on v1

--- a/solution.py
+++ b/solution.py
@@ -164,8 +164,7 @@
     du_hbm,
     dd_hbm,
     mixw_ref,
-    sgain_ref,
-    out_ref,
+    oin,
     nstate_ref,
     nconv_ref,
     tok,
@@ -185,15 +184,16 @@
     xall,
     hid,
     dhid,
-    wtab,
     part,
     part_in,
     psum,
+    diag_in,
     ret_in,
     zout,
     zin,
     oout,
-    oin,
+    wsend,
+    wrecv,
     wsem,
     bpair,
     bz_s,
@@ -208,6 +208,10 @@
     rp_r,
     re_s,
     re_r,
+    rd_s,
+    rd_r,
+    w_s,
+    w_r,
     rz_s,
     rz_r,
     o_s,
@@ -240,7 +244,7 @@
             ]
         )
     ]
-    for load in loads:
+    for load in loads[:4]:
         load.start()
 
     barrier = pltpu.get_barrier_semaphore()
@@ -256,11 +260,13 @@
         )
 
     route, rweight = routing_ref[...], rweight_ref[...]
-    for s in range(n_ep):
-        col = jnp.zeros((rows, 1), f32)
+    for d in range(n_ep):
+        row = jnp.zeros((1, rows), f32)
         for j in range(TOPK):
-            col = col + jnp.where(route[:, j : j + 1] == s, rweight[:, j : j + 1], 0.0)
-        wtab[s] = jnp.broadcast_to(col, (rows, 128)).reshape(n_tp, rr, 128)
+            row = row + jnp.where(
+                route[j : j + 1] == xor(e, d, n_ep), rweight[j : j + 1], 0.0
+            )
+        wsend[d] = jnp.broadcast_to(row, (8, rows))
 
     loads[0].wait()
     loads[1].wait()
@@ -293,9 +299,11 @@
     ) * input_gate * conv.astype(f32)
     nstate_ref[...] = new_state
     loads[2].wait()
+    loads[3].wait()
+    for load in loads[4:]:
+        load.start()
     gated = jnp.dot(tokens, gproj[...], preferred_element_type=f32).astype(bf16).astype(f32)
     mixed = (new_state * jax.nn.gelu(gated, approximate=True)).astype(bf16)
-    loads[3].wait()
     for n0 in range(0, width, wide):
         val = jnp.dot(mixed, oproj[:, n0 : n0 + wide], preferred_element_type=f32).astype(bf16)
         for j in range(n_tp):
@@ -304,6 +312,11 @@
 
     copy = remote(pmix.at[other], pmix_in, bpair.at[0], bpair.at[1], e, sibling)
     copy.start()
+    wcopies = [None]
+    for d in range(1, n_ep):
+        wc = remote(wsend.at[d], wrecv.at[d], w_s.at[d], w_r.at[d], xor(e, d, n_ep), t)
+        wc.start()
+        wcopies.append(wc)
     copy.wait_recv()
     zcopies = []
     for d in range(1, n_z):
@@ -320,120 +333,166 @@
     normed = norm_rows(mix_rows, fgain_ref[...]).astype(bf16)
     xall[e, c, k] = normed
 
-    def block(dge, dk):
+    agz, age, sib, pair = [], {}, {}, {}
+    half = n_z // 2
+
+    def slot(dge, dk):
         return xall.at[xor(e, dge, n_ep), c, xor(k, dk, n_z)]
 
-    agz, age, sib = [], {}, {}
-    own = xall.at[e, c, k]
     for d in range(1, n_z):
-        zc = remote(own, own, agz_s.at[d], agz_r.at[d], e, 2 * xor(k, d, n_z) + c)
+        zc = remote(
+            slot(0, 0), slot(0, 0), agz_s.at[d], agz_r.at[d], e, 2 * xor(k, d, n_z) + c
+        )
         zc.start()
         agz.append(zc)
 
-    def to_ep(dge, dk):
-        src = xall.at[e, c, xor(k, dk, n_z)]
-        ec = remote(src, src, age_s.at[dge, dk], age_r.at[dge, dk], xor(e, dge, n_ep), t)
+    def to_ep(dge, dk, origin=0):
+        src = slot(origin, dk)
+        at = dge ^ origin
+        ec = remote(src, src, age_s.at[at, dk], age_r.at[at, dk], xor(e, dge, n_ep), t)
         ec.start()
-        age[dge, dk] = ec
-
-    single = [d for d in range(1, n_ep) if d & (d - 1) == 0]
-    double = [d for d in range(1, n_ep) if d & (d - 1)]
-    for dge in single:
-        to_ep(dge, 0)
-    for d in range(1, n_z):
-        agz[d - 1].wait_recv()
-        for dge in single:
-            to_ep(dge, d)
-    for d in range(n_z):
-        for dge in double:
-            to_ep(dge, d)
+        age[at, dk] = ec
 
     def to_sibling(dge):
         src = xall.at[xor(e, dge, n_ep), c]
-        return remote(src, src, sib_s.at[dge], sib_r.at[dge], e, sibling)
-
-    def from_ep(dge):
-        for dk in range(n_z):
-            dst = xall.at[xor(e, dge, n_ep), c, xor(k, dk, n_z)]
-            remote(dst, dst, age_s.at[dge, dk], age_r.at[dge, dk], xor(e, dge, n_ep), t).wait_recv()
-
-    to_sibling(0).start()
-    to_sibling(0).wait_recv()
+        sib[dge] = remote(src, src, sib_s.at[dge], sib_r.at[dge], e, sibling)
+        sib[dge].start()
+
+    def forward(dk):
+        age[1, dk].wait_recv()
+        age[2, dk].wait_recv()
+        if dk < half:
+            to_ep(2, dk, 1)
+        else:
+            to_ep(1, dk, 2)
+
+    for dk in range(n_z):
+        if dk:
+            agz[dk - 1].wait_recv()
+        to_ep(1, dk)
+        to_ep(2, dk)
+    to_sibling(0)
 
     ff = eg.shape[1]
-    rows_own = xall[e].reshape(rows, width)
+    forward(0)
+    sib[0].wait_recv()
     for i in (4, 5):
         loads[i].wait()
+    rows_own = xall[e].reshape(rows, width)
     dhid[...] = (
         jax.nn.silu(jnp.dot(rows_own, dg[...], preferred_element_type=f32))
         * jnp.dot(rows_own, du[...], preferred_element_type=f32)
     ).astype(bf16)
+    for dk in range(1, n_z):
+        forward(dk)
+    to_sibling(1)
+    to_sibling(2)
     mix = jax.nn.sigmoid(
-        jnp.sum(rows_own.astype(f32) * mixw_ref[...].astype(f32), axis=1, keepdims=True)
+        jnp.sum(
+            rows_own.astype(f32) * mixw_ref[...].astype(f32).reshape(1, width),
+            axis=1,
+            keepdims=True,
+        )
     )
     for i in (6, 7, 8, 9):
         loads[i].wait()
 
-    def hidden(g):
-        x = xall[g].reshape(rows, width)
+    def hidden(dge):
+        x = xall[xor(e, dge, n_ep)].reshape(rows, width)
         for f0 in range(0, ff, 256):
             f1 = min(ff, f0 + 256)
             gate_val = jnp.dot(x, eg[:, f0:f1], preferred_element_type=f32)
             up_val = jnp.dot(x, eu[:, f0:f1], preferred_element_type=f32)
             hid[:, f0:f1] = (jax.nn.silu(gate_val) * up_val).astype(bf16)
 
-    def to_pair(dge):
-        return remote(
+    def down(dge):
+        row = (wrecv if dge else wsend)[dge][:1]
+        across = lax.broadcasted_iota(jnp.int32, (rows, rows), 0)
+        along = lax.broadcasted_iota(jnp.int32, (rows, rows), 1)
+        col = jnp.sum(jnp.where(across == along, row, 0.0), axis=1, keepdims=True)
+        weights = jnp.concatenate(
+            [col[j * rr : (j + 1) * rr] for cc in range(2) for j in range(cc, n_tp, 2)], axis=0
+        )
+        for n0 in range(0, width, wide):
+            cut = slice(n0, n0 + wide)
+            val = weights * jnp.dot(hid[...], ed[:, cut], preferred_element_type=f32)
+            if dge == 0:
+                val = val + mix * jnp.dot(dhid[...], dd[:, cut], preferred_element_type=f32)
+            part[dge, :, :, :, cut] = val.astype(bf16).reshape(2, n_z, rr, wide)
+        pair[dge] = remote(
             part.at[dge, other], part_in.at[dge], rp_s.at[dge], rp_r.at[dge], e, sibling
         )
-
-    def to_owner(dge):
-        return remote(
-            psum.at[dge], ret_in.at[dge], re_s.at[dge], re_r.at[dge], xor(e, dge, n_ep), t
-        )
-
-    hidden(e)
-    weights = jnp.concatenate(
-        [wtab[e, 2 * kk + cc][:, :1] for cc in range(2) for kk in range(n_z)], axis=0
-    )
-    for n0 in range(0, width, wide):
-        val = weights * jnp.dot(hid[...], ed[:, n0 : n0 + wide], preferred_element_type=f32)
-        val = val + mix * jnp.dot(dhid[...], dd[:, n0 : n0 + wide], preferred_element_type=f32)
-        part[0, :, :, :, n0 : n0 + wide] = val.astype(bf16).reshape(2, n_z, rr, wide)
-    to_pair(0).start()
+        pair[dge].start()
+
+    def chip_sum(dge, kk):
+        return part[dge, c, kk].astype(f32) + part_in[dge, kk].astype(f32)
+
+    blocks = {1: (0, half), 2: (half, 0)}
+    sends = []
+
+    def send(src, dst, sems, at, dge):
+        rc = remote(src, dst, sems[0].at[at], sems[1].at[at], xor(e, dge, n_ep), t)
+        rc.start()
+        sends.append(rc)
+        return rc
+
+    returns, diagonal = [], {}
 
     def finish(dge):
-        to_pair(dge).wait_recv()
-        for kk in range(n_z):
-            psum[dge, kk] = (
-                part[dge, c, kk].astype(f32) + part_in[dge, kk].astype(f32)
-            ).astype(bf16)
-        to_owner(dge).start()
-
-    def step(dge, carry):
-        from_ep(dge)
-        to_sibling(dge).start()
-        to_sibling(dge).wait_recv()
-        hidden(xor(e, dge, n_ep))
-        for n0 in range(0, width, wide):
-            val = jnp.dot(hid[...], ed[:, n0 : n0 + wide], preferred_element_type=f32)
-            part[dge, :, :, :, n0 : n0 + wide] = val.astype(bf16).reshape(2, n_z, rr, wide)
-        to_pair(dge).start()
-        finish(dge)
-        return carry
-
-    lax.fori_loop(1, n_ep, step, 0)
-
-    to_pair(0).wait_recv()
+        pair[dge].wait_recv()
+        if dge == 3:
+            for to, b0 in ((1, 0), (2, half)):
+                for kk in range(b0, b0 + half):
+                    psum[3, kk] = chip_sum(3, kk).astype(bf16)
+                cut = pl.ds(b0, half)
+                diagonal[to] = send(
+                    psum.at[3, cut], diag_in.at[cut], (rd_s, rd_r), to, to
+                )
+            return
+        b0 = blocks[dge][0]
+        for kk in range(b0, b0 + half):
+            psum[dge, kk] = chip_sum(dge, kk).astype(bf16)
+        cut = pl.ds(b0, half)
+        returns.append(
+            send(psum.at[dge, cut], ret_in.at[dge, cut], (re_s, re_r), 2 * dge, dge)
+        )
+
+    def finish_late(dge):
+        diagonal[3 - dge].wait_recv()
+        b0 = blocks[dge][1]
+        for kk in range(b0, b0 + half):
+            psum[dge, kk] = (chip_sum(dge, kk) + diag_in[kk].astype(f32)).astype(bf16)
+        cut = pl.ds(b0, half)
+        returns.append(
+            send(psum.at[dge, cut], ret_in.at[dge, cut], (re_s, re_r), 2 * dge + 1, dge)
+        )
+
+    hidden(0)
+    down(0)
     for dge in range(1, n_ep):
-        to_owner(dge).wait_recv()
+        if dge > 1:
+            for wc in [wcopies[dge]]:
+                wc.wait_recv()
+        else:
+            wcopies[1].wait_recv()
+            for dk in range(n_z):
+                age[3, dk].wait_recv()
+            to_sibling(3)
+        sib[dge].wait_recv()
+        hidden(dge)
+        if dge > 1:
+            finish(dge - 1)
+        down(dge)
+    finish(3)
+    pair[0].wait_recv()
+    finish_late(1)
+    finish_late(2)
+
+    for rc in returns:
+        rc.wait_recv()
 
     def combine(kk):
-        total = part[0, c, kk].astype(f32) + part_in[0, kk].astype(f32)
-        for dge in range(1, n_ep):
-            weight = wtab[xor(e, dge, n_ep), 2 * kk + c][:, :1]
-            total = total + weight * ret_in[dge, kk].astype(f32)
-        return total
+        return chip_sum(0, kk) + ret_in[1, kk].astype(f32) + ret_in[2, kk].astype(f32)
 
     zcopies2 = []
     for d in range(1, n_z):
@@ -460,19 +519,21 @@
     for d in range(1, n_tp):
         peer = xor(t, d, n_tp)
         remote(oout.at[peer], oin.at[peer], o_s.at[d], o_r.at[d], e, peer).wait_recv()
-    out_ref[...] = (oin[...].reshape(rows, cols) * sgain_ref[...]).astype(bf16)
 
     copy.wait_send()
-    for group in (zcopies, agz, zcopies2, ocopies):
+    for group in (zcopies, agz, wcopies[1:], sends, zcopies2, ocopies):
         for each in group:
             each.wait_send()
-    for each in age.values():
-        each.wait_send()
-    for dge in range(n_ep):
-        to_sibling(dge).wait_send()
-        to_pair(dge).wait_send()
-        if dge:
-            to_owner(dge).wait_send()
+    for group in (age, sib, pair):
+        for each in group.values():
+            each.wait_send()
+
+
+def tail_kernel(rows_ref, state_ref, conv_ref, gain_ref, out_ref, nstate_ref, nconv_ref):
+    rows, cols = out_ref.shape
+    out_ref[...] = (rows_ref[...].reshape(rows, cols) * gain_ref[...]).astype(out_ref.dtype)
+    nstate_ref[...] = state_ref[...]
+    nconv_ref[...] = conv_ref[...]
 
 
 def on_device(*args):
@@ -481,7 +542,8 @@
     n_ep, n_tp = lax.axis_size("ep"), lax.axis_size("tp")
     experts = expert_gate.shape[0] * n_ep
     capacity = max(2, 2 * rows * TOPK // experts)
-    if capacity < rows or expert_gate.shape[0] != 1 or n_ep & (n_ep - 1) or n_tp & (n_tp - 1):
+    square = n_ep == 4 and n_tp >= 4 and n_tp & (n_tp - 1) == 0
+    if capacity < rows or expert_gate.shape[0] != 1 or not square:
         return on_device_slots(*args)
     rr, n_z = rows // n_tp, n_tp // 2
     own, ff = args[3].shape[1], expert_gate.shape[2]
@@ -489,17 +551,20 @@
     operands = list(args)
     operands[0] = tokens.reshape(n_tp, rr, width)
     operands[1] = jnp.transpose(args[1], (1, 0, 2))
-    for i in (8, 10, 19, 20):
+    for i in (14, 15):
+        operands[i] = args[i].T
+    for i in (8, 10, 20):
         operands[i] = args[i].reshape(1, -1)
     for i in (11, 12, 13):
         operands[i] = args[i][0]
+    gain = operands.pop()
     in_hbm = (0, 3, 4, 9, 11, 12, 13, 16, 17, 18)
     vmem = pl.BlockSpec(memory_space=pltpu.VMEM)
     dma = pltpu.SemaphoreType.DMA
-    layer_out, new_state, new_conv = pl.pallas_call(
+    wide_out, new_state, new_conv = pl.pallas_call(
         functools.partial(block_kernel, n_ep, n_tp),
         out_shape=(
-            jax.ShapeDtypeStruct((rows, own), bf16),
+            jax.ShapeDtypeStruct((n_tp, rr, width // n_tp), f32),
             jax.ShapeDtypeStruct((rows, own), f32),
             jax.ShapeDtypeStruct((3, rows, own), bf16),
         ),
@@ -526,15 +591,16 @@
             pltpu.VMEM((n_ep, 2, n_z, rr, width), bf16),
             pltpu.VMEM((rows, ff), bf16),
             pltpu.VMEM((rows, args[16].shape[1]), bf16),
-            pltpu.VMEM((n_ep, n_tp, rr, 128), f32),
             pltpu.VMEM((n_ep, 2, n_z, rr, width), bf16),
             pltpu.VMEM((n_ep, n_z, rr, width), bf16),
             pltpu.VMEM((n_ep, n_z, rr, width), bf16),
+            pltpu.VMEM((n_z, rr, width), bf16),
             pltpu.VMEM((n_ep, n_z, rr, width), bf16),
             pltpu.VMEM((n_z, rr, width), bf16),
             pltpu.VMEM((n_z, rr, width), bf16),
             pltpu.VMEM((n_tp, rr, width // n_tp), f32),
-            pltpu.VMEM((n_tp, rr, width // n_tp), f32),
+            pltpu.VMEM((n_ep, 8, rows), f32),
+            pltpu.VMEM((n_ep, 8, rows), f32),
             dma((len(in_hbm),)),
             dma((2,)),
             dma((n_z,)),
@@ -545,6 +611,10 @@
             dma((n_ep, n_z)),
             dma((n_ep,)),
             dma((n_ep,)),
+            dma((n_ep,)),
+            dma((n_ep,)),
+            dma((2 * n_ep,)),
+            dma((2 * n_ep,)),
             dma((n_ep,)),
             dma((n_ep,)),
             dma((n_ep,)),
@@ -558,6 +628,16 @@
             collective_id=0, has_side_effects=True, vmem_limit_bytes=56 * 2**20
         ),
     )(*operands)
+    layer_out, new_state, new_conv = pl.pallas_call(
+        tail_kernel,
+        out_shape=(
+            jax.ShapeDtypeStruct((rows, own), bf16),
+            jax.ShapeDtypeStruct((rows, own), f32),
+            jax.ShapeDtypeStruct((3, rows, own), bf16),
+        ),
+        in_specs=[vmem] * 4,
+        out_specs=(vmem,) * 3,
+    )(wide_out, new_state, new_conv, gain)
     return layer_out, new_state, jnp.transpose(new_conv, (1, 0, 2))
 
 

time: 72.8 us -> 64.6 us (0.89)
  local copies, waits for them, and re-layouts: 8.77 us -> 0 us
    unnamed x5 -> x0, local copies, waits for them, and re-layouts: 7.48 us -> none
    pallas_call x0 -> x1, Pallas kernels: none -> 1.81 us  [on_device(): pl.pallas_call(tail_kernel, out_shape=(jax.ShapeDtypeStruct((rows, own),...]
    reshape x1 -> x0, local copies, waits for them, and re-layouts: 1.29 us -> none  [on_device(): operands[i] = args[i].reshape(1, -1)]
    pallas_call x1, Pallas kernels: 63.1 us -> 62 us  [on_device(): pl.pallas_call(functools.partial(block_kernel, n_ep, n_tp), out_shape=(ja...]
where the time goes in v2:
time: 64.6 us; the launch traced here: 64.5 us
  Pallas kernels  63.8 us (99%)
  between operations  0.65 us (1%)
    pallas_call x1, Pallas kernels, on_device(): pl.pallas_call(functools.partial(block_kernel, n_ep, n_tp), out_shape=(ja...  62 us
    pallas_call x1, Pallas kernels, on_device(): pl.pallas_call(tail_kernel, out_shape=(jax.ShapeDtypeStruct((rows, own),...  1.81 us

profile of v2, /device:TPU:0, one launch (start us, length us, event | category | flops | bytes accessed | tf_op | source)
XLA Modules:
  0.0 64.5 jit_solution(3834526984898042142)
XLA Ops:
  0.6 62.0 %shard_map.220 = (f32[8,16,256]{2,1,0:T(8,128)}, f32[128,256]{1,0:T(8,128)}, bf16[3,128,256]{2,1,0:T(8,128)(2,1)}) custom-call(bf16[8,16,2048]{2,1,0:T(8,128)(2,1)} %bitcast.14, bf16[3,128,256]{2,1,0:T(8,128)(2,1)} %bitcast.15, f32[128,256]{1,0:T(8,128)} %state_ref.1, bf16[2048,256]{1,0:T(8,128)(2,1)} %gproj_hbm.1, bf16[2048,256]{1,0:T(8,128)(2,1)} %iproj_hbm.1, ...), custom_call_target="tpu_custom_call" | custom-call | tf_op jit(solution)/shard_map/pallas_call | solution.py:564
  62.6 1.8 %shard_map.221 = (bf16[128,256]{1,0:T(8,128)(2,1)}, f32[128,256]{1,0:T(8,128)}, bf16[3,128,256]{2,1,0:T(8,128)(2,1)}) custom-call(f32[8,16,256]{2,1,0:T(8,128)} %get-tuple-element.9.rows_ref, f32[128,256]{1,0:T(8,128)} %get-tuple-element.10.state_ref, bf16[3,128,256]{2,1,0:T(8,128)(2,1)} %get-tuple-element.11.conv_ref, f32[1,256]{1,0:T(1,128)} %bitcast.20), custom_call_target="tpu_custom_call" | custom-call | tf_op jit(solution)/shard_map/pallas_call | solution.py:631

commit v3 on v2

--- a/solution.py
+++ b/solution.py
@@ -427,81 +427,77 @@
     def chip_sum(dge, kk):
         return part[dge, c, kk].astype(f32) + part_in[dge, kk].astype(f32)
 
-    blocks = {1: (0, half), 2: (half, 0)}
+    order = list(range(1, n_z)) + [0]
+    by_first, by_second = order[0::2], order[1::2]
+    early = {1: by_first, 2: by_second}
     sends = []
 
-    def send(src, dst, sems, at, dge):
-        rc = remote(src, dst, sems[0].at[at], sems[1].at[at], xor(e, dge, n_ep), t)
+    def send(src, dst, send_sem, recv_sem, dge):
+        rc = remote(src, dst, send_sem, recv_sem, xor(e, dge, n_ep), t)
         rc.start()
         sends.append(rc)
         return rc
 
-    returns, diagonal = [], {}
+    returns, diagonal = {}, {}
+
+    def to_owner(dge, dk):
+        returns[dge, dk] = send(
+            psum.at[dge, dk], ret_in.at[dge, dk], re_s.at[dge, dk], re_r.at[dge, dk], dge
+        )
 
     def finish(dge):
         pair[dge].wait_recv()
-        if dge == 3:
-            for to, b0 in ((1, 0), (2, half)):
-                for kk in range(b0, b0 + half):
-                    psum[3, kk] = chip_sum(3, kk).astype(bf16)
-                cut = pl.ds(b0, half)
-                diagonal[to] = send(
-                    psum.at[3, cut], diag_in.at[cut], (rd_s, rd_r), to, to
+        for dk in order if dge == 3 else early[dge]:
+            psum[dge, dk] = chip_sum(dge, xor(k, dk, n_z)).astype(bf16)
+            if dge == 3:
+                diagonal[dk] = send(
+                    psum.at[3, dk],
+                    diag_in.at[dk],
+                    rd_s.at[dk],
+                    rd_r.at[dk],
+                    1 if dk in by_first else 2,
                 )
-            return
-        b0 = blocks[dge][0]
-        for kk in range(b0, b0 + half):
-            psum[dge, kk] = chip_sum(dge, kk).astype(bf16)
-        cut = pl.ds(b0, half)
-        returns.append(
-            send(psum.at[dge, cut], ret_in.at[dge, cut], (re_s, re_r), 2 * dge, dge)
-        )
-
-    def finish_late(dge):
-        diagonal[3 - dge].wait_recv()
-        b0 = blocks[dge][1]
-        for kk in range(b0, b0 + half):
-            psum[dge, kk] = (chip_sum(dge, kk) + diag_in[kk].astype(f32)).astype(bf16)
-        cut = pl.ds(b0, half)
-        returns.append(
-            send(psum.at[dge, cut], ret_in.at[dge, cut], (re_s, re_r), 2 * dge + 1, dge)
-        )
-
-    hidden(0)
-    down(0)
+            else:
+                to_owner(dge, dk)
+
     for dge in range(1, n_ep):
-        if dge > 1:
-            for wc in [wcopies[dge]]:
-                wc.wait_recv()
-        else:
-            wcopies[1].wait_recv()
+        wcopies[dge].wait_recv()
+        sib[dge].wait_recv()
+        hidden(dge)
+        if dge == 2:
             for dk in range(n_z):
                 age[3, dk].wait_recv()
             to_sibling(3)
-        sib[dge].wait_recv()
-        hidden(dge)
         if dge > 1:
             finish(dge - 1)
         down(dge)
     finish(3)
+    hidden(0)
+    down(0)
+    for dk in order:
+        dge = 2 if dk in by_first else 1
+        diagonal[dk].wait_recv()
+        psum[dge, dk] = (
+            chip_sum(dge, xor(k, dk, n_z)) + diag_in[dk].astype(f32)
+        ).astype(bf16)
+        to_owner(dge, dk)
     pair[0].wait_recv()
-    finish_late(1)
-    finish_late(2)
-
-    for rc in returns:
-        rc.wait_recv()
-
-    def combine(kk):
-        return chip_sum(0, kk) + ret_in[1, kk].astype(f32) + ret_in[2, kk].astype(f32)
+
+    def combine(dk):
+        returns[1, dk].wait_recv()
+        returns[2, dk].wait_recv()
+        return (
+            chip_sum(0, xor(k, dk, n_z)) + ret_in[1, dk].astype(f32) + ret_in[2, dk].astype(f32)
+        )
 
     zcopies2 = []
     for d in range(1, n_z):
         kk = xor(k, d, n_z)
-        zout[d] = combine(kk).astype(bf16)
+        zout[d] = combine(d).astype(bf16)
         zc = remote(zout.at[d], zin.at[d], rz_s.at[d], rz_r.at[d], e, 2 * kk + c)
         zc.start()
         zcopies2.append(zc)
-    total = combine(k) + ALPHA * xall[e, c, k].astype(f32)
+    total = combine(0) + ALPHA * xall[e, c, k].astype(f32)
     for d in range(1, n_z):
         zcopies2[d - 1].wait_recv()
         total = total + zin[d].astype(f32)
@@ -613,10 +609,10 @@
             dma((n_ep,)),
             dma((n_ep,)),
             dma((n_ep,)),
-            dma((2 * n_ep,)),
-            dma((2 * n_ep,)),
-            dma((n_ep,)),
-            dma((n_ep,)),
+            dma((n_ep, n_z)),
+            dma((n_ep, n_z)),
+            dma((n_z,)),
+            dma((n_z,)),
             dma((n_ep,)),
             dma((n_ep,)),
             dma((n_z,)),

time: 64.6 us -> 60.2 us (0.932)
  Pallas kernels: 63.8 us -> 59.4 us
    pallas_call x1, Pallas kernels: 62 us -> 57.6 us  [on_device(): pl.pallas_call(functools.partial(block_kernel, n_ep, n_tp), out_shape=(ja...]
where the time goes in v3:
time: 60.2 us; the launch traced here: 60 us
  Pallas kernels  59.4 us (99%)
  between operations  0.65 us (1%)
    pallas_call x1, Pallas kernels, on_device(): pl.pallas_call(functools.partial(block_kernel, n_ep, n_tp), out_shape=(ja...  57.6 us
    pallas_call x1, Pallas kernels, on_device(): pl.pallas_call(tail_kernel, out_shape=(jax.ShapeDtypeStruct((rows, own),...  1.81 us

profile of v3, /device:TPU:0, one launch (start us, length us, event | category | flops | bytes accessed | tf_op | source)
XLA Modules:
  0.0 60.0 jit_solution(16314934731596165779)
XLA Ops:
  0.6 57.6 %shard_map.220 = (f32[8,16,256]{2,1,0:T(8,128)}, f32[128,256]{1,0:T(8,128)}, bf16[3,128,256]{2,1,0:T(8,128)(2,1)}) custom-call(bf16[8,16,2048]{2,1,0:T(8,128)(2,1)} %bitcast.14, bf16[3,128,256]{2,1,0:T(8,128)(2,1)} %bitcast.15, f32[128,256]{1,0:T(8,128)} %state_ref.1, bf16[2048,256]{1,0:T(8,128)(2,1)} %gproj_hbm.1, bf16[2048,256]{1,0:T(8,128)(2,1)} %iproj_hbm.1, ...), custom_call_target="tpu_custom_call" | custom-call | tf_op jit(solution)/shard_map/pallas_call | solution.py:560
  58.2 1.8 %shard_map.221 = (bf16[128,256]{1,0:T(8,128)(2,1)}, f32[128,256]{1,0:T(8,128)}, bf16[3,128,256]{2,1,0:T(8,128)(2,1)}) custom-call(f32[8,16,256]{2,1,0:T(8,128)} %get-tuple-element.9.rows_ref, f32[128,256]{1,0:T(8,128)} %get-tuple-element.10.state_ref, bf16[3,128,256]{2,1,0:T(8,128)(2,1)} %get-tuple-element.11.conv_ref, f32[1,256]{1,0:T(1,128)} %bitcast.20), custom_call_target="tpu_custom_call" | custom-call | tf_op jit(solution)/shard_map/pallas_call | solution.py:627
